TPU v7x, 128 devices: a whole 4x4x4 slice. The times are simulated.
128 devices in a mesh: ep: 64 (over z, y, x), tp: 2 (over core).
Axes of the slice: x: 4, y: 4, z: 4, core: 2. Of those that a mesh axis runs over, the one named last changes fastest.
Arguments:
- tokens: bfloat16 [16384, 4096], P('ep'), may hold values from -6 to 6
- cotangent: bfloat16 [16384, 4096], P('ep'), may hold values from -1.5 to 1.5
- gates: float32 [16384, 2], P('ep'), may hold values from 0.05 to 0.95
- experts: int32 [16384, 2], P('ep'), may hold values from 0 to 63, all different within a row; in each aligned block of 256 rows (0 to 255, 256 to 511, ...) at most 12 rows name the same one
- gate_w: bfloat16 [64, 4096, 768], P('ep', None, 'tp'), may hold values from -0.09375 to 0.09375
- up_w: bfloat16 [64, 4096, 768], P('ep', None, 'tp'), may hold values from -0.09375 to 0.09375
- down_w: bfloat16 [64, 768, 4096], P('ep', 'tp'), may hold values from -0.21875 to 0.21875
Outputs:
- grad_tokens: bfloat16 [16384, 4096], P('ep', 'tp')
- grad_gates: float32 [16384, 2], P('ep')
- grad_gate_w: bfloat16 [64, 4096, 768], P('ep', None, 'tp')
- grad_up_w: bfloat16 [64, 4096, 768], P('ep', None, 'tp')
- grad_down_w: bfloat16 [64, 768, 4096], P('ep', 'tp')
- sq_gate: float32 [64, 4096], P('ep')
- sq_up: float32 [64, 4096], P('ep')
- sq_down: float32 [64, 768], P('ep', 'tp')
Inputs may be any that keep to these rules, and one draw needn't show every extreme that they name: In each aligned block of 256 rows no expert is named by more than 12 rows, a bound that some expert reaches in some blocks; the 2 experts of a row differ.
All inputs are finite; a program needn't handle non-finite values.
Results may differ from a plain program's by a relative error of at most 0.024.
Values may be sent and summed in bfloat16 or wider, within the bound.
A program may use at most 192 MiB of HBM per device.

v0:
```python
import jax
import jax.numpy as jnp
from jax import lax
from jax.sharding import PartitionSpec as P


def in_blocks(array, dim, peers):
    dims = array.shape
    blocks = array.reshape(*dims[:dim], peers, dims[dim] // peers, *dims[dim + 1 :])
    return jnp.moveaxis(blocks, dim, 0)


def summed_on_arrival(array, axis, dim):
    peers = lax.axis_size(axis)
    blocks = lax.all_to_all(in_blocks(array, dim, peers), axis, 0, 0, tiled=True)
    return jnp.sum(blocks.astype(jnp.float32), axis=0)


def body(tokens, cotangent, gates, experts, gate_w, up_w, down_w):
    tok_rows = tokens.shape[0]
    top_count = experts.shape[1]
    width = tokens.shape[1]
    n_ep = lax.axis_size("ep")
    capacity = 3 * tok_rows * top_count // (2 * n_ep)
    n_slots = n_ep * capacity
    flat_ids = experts.reshape(-1)
    onehot = (flat_ids[:, None] == jnp.arange(n_ep, dtype=jnp.int32)[None, :]).astype(jnp.int32)
    earlier = jnp.cumsum(onehot, axis=0) - onehot
    slot_of = jnp.sum(earlier * onehot, axis=1)
    target = flat_ids * capacity + slot_of
    placing = (target[None, :] == jnp.arange(n_slots, dtype=jnp.int32)[:, None]).astype(jnp.float32)
    place_tok = jnp.sum(placing.reshape(n_slots, tok_rows, top_count), axis=2).astype(jnp.bfloat16)
    send_gate = jnp.dot(placing, gates.reshape(-1), precision=lax.Precision.HIGHEST)
    n_cores = lax.axis_size("tp")
    share = width // n_cores
    offset = lax.axis_index("tp") * share
    tok_share = lax.dynamic_slice_in_dim(tokens, offset, share, 1)
    cot_share = lax.dynamic_slice_in_dim(cotangent, offset, share, 1)
    send_x = jnp.dot(place_tok, tok_share, preferred_element_type=jnp.float32).astype(jnp.bfloat16)
    send_dy = jnp.dot(place_tok, cot_share, preferred_element_type=jnp.float32).astype(jnp.bfloat16)
    part_x, part_dy, recv_gate = (
        lax.all_to_all(
            send_x.reshape(n_ep, capacity, share), "ep", split_axis=0, concat_axis=0, tiled=True
        ),
        lax.all_to_all(
            send_dy.reshape(n_ep, capacity, share), "ep", split_axis=0, concat_axis=0, tiled=True
        ),
        lax.all_to_all(
            send_gate.reshape(n_ep, capacity).astype(jnp.bfloat16),
            "ep",
            split_axis=0,
            concat_axis=0,
            tiled=True,
        ).astype(jnp.float32),
    )
    stacked = jnp.stack([part_x, part_dy], axis=0)
    joined = lax.all_gather(stacked, "tp", axis=3, tiled=True)
    recv_x = joined[0]
    recv_dy = joined[1]
    recv_x = recv_x.reshape(n_slots, width)
    recv_dy = recv_dy.reshape(n_slots, width)
    recv_gate = recv_gate.reshape(n_slots)
    w_gate = gate_w[0]
    w_up = up_w[0]
    w_down = down_w[0]
    contract_last = (((1,), (1,)), ((), ()))
    contract_first = (((0,), (0,)), ((), ()))
    pre_gate = jnp.dot(recv_x, w_gate, preferred_element_type=jnp.float32)
    pre_up = jnp.dot(recv_x, w_up, preferred_element_type=jnp.float32)
    sigmoid_gate = jax.nn.sigmoid(pre_gate)
    silu_gate = pre_gate * sigmoid_gate
    hidden = (silu_gate * pre_up).astype(jnp.bfloat16)
    hidden_grad = lax.dot_general(
        recv_dy, w_down, contract_last, preferred_element_type=jnp.float32
    )
    gate_part = jnp.sum(hidden.astype(jnp.float32) * hidden_grad, axis=1)
    scaled = recv_gate[:, None] * hidden_grad
    grad_pre_gate = (
        scaled * pre_up * sigmoid_gate * (1.0 + pre_gate * (1.0 - sigmoid_gate))
    ).astype(jnp.bfloat16)
    grad_pre_up = (scaled * silu_gate).astype(jnp.bfloat16)
    weighted = (recv_gate[:, None] * hidden.astype(jnp.float32)).astype(jnp.bfloat16)
    grad_dw = lax.dot_general(
        weighted, recv_dy, contract_first, preferred_element_type=jnp.float32
    ).astype(jnp.bfloat16)
    grad_gw = lax.dot_general(
        recv_x, grad_pre_gate, contract_first, preferred_element_type=jnp.float32
    ).astype(jnp.bfloat16)
    grad_uw = lax.dot_general(
        recv_x, grad_pre_up, contract_first, preferred_element_type=jnp.float32
    ).astype(jnp.bfloat16)
    partial_value = lax.dot_general(
        grad_pre_gate, w_gate, contract_last, preferred_element_type=jnp.float32
    ) + lax.dot_general(grad_pre_up, w_up, contract_last, preferred_element_type=jnp.float32)
    partial_terms = partial_value.astype(jnp.bfloat16).astype(jnp.float32)
    gate_total = lax.psum(gate_part, "tp")
    summed = summed_on_arrival(partial_terms.astype(jnp.bfloat16), "tp", 1)
    half_width = summed.shape[1]
    row_grad = summed.astype(jnp.bfloat16)
    back_rows, back_gate = (
        lax.all_to_all(
            row_grad.reshape(n_ep, capacity, half_width),
            "ep",
            split_axis=0,
            concat_axis=0,
            tiled=True,
        ),
        lax.all_to_all(
            gate_total.reshape(n_ep, capacity).astype(jnp.bfloat16),
            "ep",
            split_axis=0,
            concat_axis=0,
            tiled=True,
        ).astype(jnp.float32),
    )
    home_rows = back_rows.reshape(n_slots, half_width)
    grad_tokens = lax.dot_general(
        place_tok, home_rows, contract_first, preferred_element_type=jnp.float32
    ).astype(jnp.bfloat16)
    grad_gates = jnp.dot(
        back_gate.reshape(n_slots), placing, precision=lax.Precision.HIGHEST
    ).reshape(tok_rows, top_count)
    gw_f = grad_gw.astype(jnp.float32)
    uw_f = grad_uw.astype(jnp.float32)
    dw_f = grad_dw.astype(jnp.float32)
    sq_gate_part = jnp.sum(gw_f * gw_f, axis=1)
    sq_up_part = jnp.sum(uw_f * uw_f, axis=1)
    sq_gate, sq_up = (
        lax.psum(sq_gate_part.astype(jnp.bfloat16), "tp").astype(jnp.float32),
        lax.psum(sq_up_part.astype(jnp.bfloat16), "tp").astype(jnp.float32),
    )
    full_units = w_gate.shape[1] * lax.axis_size("tp")
    sq_gate = sq_gate / full_units
    sq_up = sq_up / full_units
    sq_down = jnp.sum(dw_f * dw_f, axis=1) / width
    return (
        grad_tokens,
        grad_gates,
        grad_gw[None],
        grad_uw[None],
        grad_dw[None],
        sq_gate[None],
        sq_up[None],
        sq_down[None],
    )


def solution(mesh):
    placed = (
        P("ep", None),
        P("ep", None),
        P("ep", None),
        P("ep", None),
        P("ep", None, "tp"),
        P("ep", None, "tp"),
        P("ep", "tp", None),
    )
    return jax.shard_map(
        body,
        mesh=mesh,
        in_specs=placed,
        out_specs=(
            P("ep", "tp"),
            P("ep", None),
            P("ep", None, "tp"),
            P("ep", None, "tp"),
            P("ep", "tp", None),
            P("ep", None),
            P("ep", None),
            P("ep", "tp"),
        ),
        check_vma=False,
    )
```

profile of v0, /device:TPU:88, one launch (start us, length us, event | category | flops | bytes accessed | tf_op | source)
XLA Modules:
  0.0 352.8 jit_solution(4803455188419291347)
XLA Ops:
  15.2 6.1 %reshape.147 = bf16[64,12,2048]{2,1,0:T(8,128)(2,1)} reshape(bf16[768,2048]{1,0:T(8,128)(2,1)} %convolution_convert_fusion.3) | data formatting | bytes 6291456 | tf_op jit(solution)/shard_map/reshape | solution.py:46
  21.3 10.6 %all-to-all-start.2 = ((bf16[64,12,2048]{2,1,0:T(8,128)(2,1)}), bf16[64,12,2048]{2,1,0:T(8,128)(2,1)}, u32[]{:S(2)}, u32[]{:S(2)}) async-start(bf16[64,12,2048]{2,1,0:T(8,128)(2,1)} %reshape.147), calls=%async_computation.2 | async-start | bytes 8388608 | tf_op jit(solution)/shard_map/all_to_all | solution.py:45
  35.9 6.1 %reshape.146 = bf16[64,12,2048]{2,1,0:T(8,128)(2,1)} reshape(bf16[768,2048]{1,0:T(8,128)(2,1)} %convolution_convert_fusion.4) | data formatting | bytes 6291456 | tf_op jit(solution)/shard_map/reshape | solution.py:43
  42.0 39.7 %all-to-all-done.2 = bf16[64,12,2048]{2,1,0:T(8,128)(2,1)} async-done(((bf16[64,12,2048]{2,1,0:T(8,128)(2,1)}), bf16[64,12,2048]{2,1,0:T(8,128)(2,1)}, u32[]{:S(2)}, u32[]{:S(2)}) %all-to-all-start.2) | async-done | bytes 3145760 | tf_op jit(solution)/shard_map/all_to_all | solution.py:45
  81.6 61.8 %all_to_all.35 = bf16[64,12,2048]{2,1,0:T(8,128)(2,1)} all-to-all(bf16[64,12,2048]{2,1,0:T(8,128)(2,1)} %reshape.146), channel_id=1, replica_groups=mesh['ep'=64,'tp'=2] {'ep'}, dimensions={0} | all-to-all | bytes 6291456 | tf_op jit(solution)/shard_map/all_to_all | solution.py:42
  143.4 7.8 %pad_maximum_fusion = bf16[2,64,12,2048]{3,2,1,0:T(8,128)(2,1)} fusion(bf16[1,64,12,2048]{3,2,1,0:T(8,128)(2,1)} %bitcast.4, bf16[1,64,12,2048]{3,2,1,0:T(8,128)(2,1)} %bitcast.76), kind=kLoop, calls=%fused_computation.1 | loop fusion | flops 3145728 | bytes 12582912 | tf_op jit(solution)/shard_map/stack | solution.py:56
  157.6 16.0 %all_to_all.36 = bf16[64,1,12]{2,1,0:T(2,128)(2,1)S(1)} all-to-all(bf16[64,1,12]{2,1,0:T(2,128)(2,1)} %copy.69), channel_id=1, replica_groups=mesh['ep'=64,'tp'=2] {'ep'}, dimensions={0} | all-to-all | bytes 3072 | tf_op jit(solution)/shard_map/all_to_all | solution.py:48
  175.1 10.0 %all-gather.2.cloned.1.call-done = bf16[2,64,12,4096]{3,2,1,0:T(8,128)(2,1)} async-done(((bf16[2,64,12,2048]{3,2,1,0:T(8,128)(2,1)}), bf16[2,64,12,4096]{3,2,1,0:T(8,128)(2,1)}) %all-gather.2.cloned.1.call-update) | async-done | bytes 12582928 | tf_op jit(solution)/shard_map/all_gather | solution.py:57
  185.1 11.7 %fusion.32 = (bf16[1,64,12,4096]{3,2,1,0:T(8,128)(2,1)}, bf16[1,64,12,4096]{3,2,1,0:T(8,128)(2,1)}) fusion(bf16[2,64,12,4096]{3,2,1,0:T(8,128)(2,1)} %all-gather.2.cloned.1.call-done), kind=kLoop, calls=%fused_computation.65 | loop fusion | bytes 25165824 | tf_op jit(solution)/shard_map/slice | solution.py:59
  196.8 9.9 %reshape_squeeze.6 = bf16[768,4096]{1,0:T(8,128)(2,1)} reshape(bf16[1,64,12,4096]{3,2,1,0:T(8,128)(2,1)} %get-tuple-element.60) | data formatting | bytes 12582912 | tf_op jit(solution)/shard_map/reshape;squeeze | solution.py:61
  206.7 9.9 %reshape_squeeze.7 = bf16[768,4096]{1,0:T(8,128)(2,1)} reshape(bf16[1,64,12,4096]{3,2,1,0:T(8,128)(2,1)} %get-tuple-element.61) | data formatting | bytes 12582912 | tf_op jit(solution)/shard_map/reshape;squeeze | solution.py:60
  216.5 5.6 %fusion.2 = f32[768,384]{0,1:T(8,128)S(1)} fusion(bf16[768,4096]{1,0:T(8,128)(2,1)} %reshape_squeeze.7, bf16[1,4096,384]{2,1,0:T(8,128)(2,1)S(1)} %copy-done), kind=kOutput, calls=%fused_computation.13 | convolution fusion | flops 2415919104 | bytes 10616832 | tf_op jit(solution)/shard_map/dot_general | solution.py:68
  225.0 4.3 %fusion.14 = (f32[768]{0:T(1024)S(1)}, bf16[768,384]{0,1:T(8,128)(2,1)}, bf16[768,384]{0,1:T(8,128)(2,1)}, bf16[768,384]{0,1:T(8,128)(2,1)}) fusion(f32[768,384]{0,1:T(8,128)S(1)} %fusion.5, f32[768,384]{0,1:T(8,128)S(1)} %fusion.2, f32[768]{0:T(1024)S(1)} %reshape.152, bf16[768,4096]{1,0:T(8,128)(2,1)S(1)} %bitcast.78, bf16[1,384,4096]{2,1,0:T(8,128)(2,1)S(1)} %copy-done.8), kind=kOutput, calls=%fused_computation.30 | convolution fusion | flops 2421521664 | bytes 13572096 | tf_op jit(solution)/shard_map/dot_general | solution.py:73
  232.7 7.6 %fusion = f32[768,4096]{1,0:T(8,128)} fusion(bf16[768,384]{0,1:T(8,128)(2,1)} %get-tuple-element.62, bf16[1,4096,384]{2,1,0:T(8,128)(2,1)S(1)} %copy-done), kind=kOutput, calls=%fused_computation.11 | convolution fusion | flops 2415919104 | bytes 16318464 | tf_op jit(solution)/shard_map/dot_general | solution.py:92
  240.3 6.6 %add_convert_fusion = bf16[768,4096]{1,0:T(8,128)(2,1)S(1)} fusion(f32[768,4096]{1,0:T(8,128)} %fusion, bf16[768,384]{0,1:T(8,128)(2,1)S(1)} %copy-done.5, bf16[1,4096,384]{2,1,0:T(8,128)(2,1)S(1)} %copy-done.4), kind=kOutput, calls=%fused_computation | convolution fusion | flops 2422210560 | bytes 22609920 | tf_op jit(solution)/shard_map/dot_general | solution.py:94
  248.0 10.0 %all_to_all.37 = bf16[2,768,2048]{2,1,0:T(8,128)(2,1)} all-to-all(bf16[2,768,2048]{2,1,0:T(8,128)(2,1)S(1)} %bitcast.74), channel_id=1, replica_groups=mesh['ep'=64,'tp'=2] {'tp'}, dimensions={0} | all-to-all | bytes 12582912 | tf_op jit(solution)/shard_map/all_to_all | solution.py:15
  258.0 10.5 %all-to-all-start.5 = ((bf16[64,1,12]{2,1,0:T(2,128)(2,1)}), bf16[64,1,12]{2,1,0:T(2,128)(2,1)}, u32[]{:S(2)}, u32[]{:S(2)}) async-start(bf16[64,1,12]{2,1,0:T(2,128)(2,1)} %convert_element_type.132), calls=%async_computation.5 | async-start | bytes 65536 | tf_op jit(solution)/shard_map/all_to_all | solution.py:108
  268.5 5.3 %reduce_sum.71 = bf16[768,2048]{1,0:T(8,128)(2,1)S(1)} reduce(bf16[2,768,2048]{2,1,0:T(8,128)(2,1)} %all_to_all.37, bf16[]{:T(256)} %constant.27.clone.1), dimensions={0}, to_apply=%region_4.5 | reduce | flops 1572864 | bytes 9437186 | tf_op jit(solution)/shard_map/reduce_sum | solution.py:16
  276.5 10.7 %all-to-all-start.4 = ((bf16[64,12,2048]{2,1,0:T(8,128)(2,1)}), bf16[64,12,2048]{2,1,0:T(8,128)(2,1)}, u32[]{:S(2)}, u32[]{:S(2)}) async-start(bf16[64,12,2048]{2,1,0:T(8,128)(2,1)} %reshape.149), calls=%async_computation.4 | async-start | bytes 8388608 | tf_op jit(solution)/shard_map/all_to_all | solution.py:101
  287.2 7.1 %multiply_reduce_fusion = (f32[384]{0:T(512)S(1)}, bf16[384,4096]{1,0:T(8,128)(2,1)}) fusion(bf16[768,4096]{1,0:T(8,128)(2,1)} %reshape_squeeze.6, bf16[768,384]{0,1:T(8,128)(2,1)S(1)} %copy-done.9, f32[768]{0:T(1024)S(1)} %reshape.152), kind=kOutput, calls=%fused_computation.3 | convolution fusion | flops 2423094784 | bytes 10031616 | tf_op jit(solution)/shard_map/dot_general | solution.py:83
  294.9 5.6 %multiply_reduce_fusion.1 = (bf16[4096]{0:T(1024)(128)(2,1)S(1)}, bf16[4096,384]{0,1:T(8,128)(2,1)S(1)}) fusion(bf16[768,384]{0,1:T(8,128)(2,1)S(1)} %copy-done.6, bf16[768,4096]{1,0:T(8,128)(2,1)} %reshape_squeeze.7), kind=kOutput, calls=%fused_computation.4 | convolution fusion | flops 2422206464 | bytes 10035200 | tf_op jit(solution)/shard_map/dot_general | solution.py:89
  303.3 6.2 %multiply_reduce_fusion.2 = (bf16[4096]{0:T(1024)(128)(2,1)}, bf16[4096,384]{0,1:T(8,128)(2,1)S(1)}) fusion(bf16[768,384]{0,1:T(8,128)(2,1)} %get-tuple-element.62, bf16[768,4096]{1,0:T(8,128)(2,1)} %reshape_squeeze.7), kind=kOutput, calls=%fused_computation.5 | convolution fusion | flops 2422206464 | bytes 10035200 | tf_op jit(solution)/shard_map/dot_general | solution.py:86
  319.0 16.8 %all-to-all-done.4 = bf16[64,12,2048]{2,1,0:T(8,128)(2,1)} async-done(((bf16[64,12,2048]{2,1,0:T(8,128)(2,1)}), bf16[64,12,2048]{2,1,0:T(8,128)(2,1)}, u32[]{:S(2)}, u32[]{:S(2)}) %all-to-all-start.4) | async-done | bytes 3145760 | tf_op jit(solution)/shard_map/all_to_all | solution.py:101
  335.8 6.3 %reshape.150 = bf16[768,2048]{1,0:T(8,128)(2,1)} reshape(bf16[64,12,2048]{2,1,0:T(8,128)(2,1)} %all-to-all-done.4) | data formatting | bytes 6291456 | tf_op jit(solution)/shard_map/reshape | solution.py:116
  (70 shorter events, 46.5 us)
Async XLA Ops:
  7.2 209.3 %copy-start = (bf16[1,4096,384]{2,1,0:T(8,128)(2,1)S(1)}, bf16[1,4096,384]{2,1,0:T(8,128)(2,1)}, u32[]{:S(2)}) copy-start(bf16[1,4096,384]{2,1,0:T(8,128)(2,1)} %param.11) | copy-start | bytes 9437188
  21.3 60.3 %all-to-all-start.2 = ((bf16[64,12,2048]{2,1,0:T(8,128)(2,1)}), bf16[64,12,2048]{2,1,0:T(8,128)(2,1)}, u32[]{:S(2)}, u32[]{:S(2)}) async-start(bf16[64,12,2048]{2,1,0:T(8,128)(2,1)} %reshape.147), calls=%async_computation.2 | async-start | bytes 8388608 | tf_op jit(solution)/shard_map/all_to_all | solution.py:45
  31.9 153.1 %all-gather.2.cloned.1.call-start = ((), (), s32[]{:S(2)}) async-start(), calls=%async_computation.6 | async-start | bytes 25165824 | tf_op jit(solution)/shard_map/all_gather | solution.py:57
  151.2 0.7 copy-start.7
  216.5 5.6 %copy-start.2 = (bf16[768,4096]{1,0:T(8,128)(2,1)S(1)}, bf16[768,4096]{1,0:T(8,128)(2,1)}, u32[]{:S(2)}) copy-start(bf16[768,4096]{1,0:T(8,128)(2,1)} %reshape_squeeze.7) | copy-start | bytes 18874372
  216.5 5.6 %copy-start.3 = (bf16[1,4096,384]{2,1,0:T(8,128)(2,1)S(1)}, bf16[1,4096,384]{2,1,0:T(8,128)(2,1)}, u32[]{:S(2)}) copy-start(bf16[1,4096,384]{2,1,0:T(8,128)(2,1)} %param.12) | copy-start | bytes 9437188
  216.5 8.3 %slice-start = ((s8[6291456]{0:T(1024)(128)(4,1)}), s8[4194304]{0:T(1024)(128)(4,1)S(1)}, s32[]{:S(2)}) async-start(s8[6291456]{0:T(1024)(128)(4,1)} %bitcast.77), calls=%async_computation.7 | async-start | bytes 8388608
  222.1 2.7 slice-start.1
  222.1 2.8 copy-start.8
  232.7 7.6 %copy-start.4 = (bf16[1,4096,384]{2,1,0:T(8,128)(2,1)S(1)}, bf16[1,4096,384]{2,1,0:T(8,128)(2,1)}, u32[]{:S(2)}) copy-start(bf16[1,4096,384]{2,1,0:T(8,128)(2,1)} %param.12) | copy-start | bytes 9437188
  232.7 7.6 %copy-start.5 = (bf16[768,384]{0,1:T(8,128)(2,1)S(1)}, bf16[768,384]{0,1:T(8,128)(2,1)}, u32[]{:S(2)}) copy-start(bf16[768,384]{0,1:T(8,128)(2,1)} %get-tuple-element.63) | copy-start | bytes 1769476
  258.0 18.5 %all-to-all-start.5 = ((bf16[64,1,12]{2,1,0:T(2,128)(2,1)}), bf16[64,1,12]{2,1,0:T(2,128)(2,1)}, u32[]{:S(2)}, u32[]{:S(2)}) async-start(bf16[64,1,12]{2,1,0:T(2,128)(2,1)} %convert_element_type.132), calls=%async_computation.5 | async-start | bytes 65536 | tf_op jit(solution)/shard_map/all_to_all | solution.py:108
  276.5 10.7 %copy-start.9 = (bf16[768,384]{0,1:T(8,128)(2,1)S(1)}, bf16[768,384]{0,1:T(8,128)(2,1)}, u32[]{:S(2)}) copy-start(bf16[768,384]{0,1:T(8,128)(2,1)} %get-tuple-element.59) | copy-start | bytes 1769476
  276.5 59.3 %all-to-all-start.4 = ((bf16[64,12,2048]{2,1,0:T(8,128)(2,1)}), bf16[64,12,2048]{2,1,0:T(8,128)(2,1)}, u32[]{:S(2)}, u32[]{:S(2)}) async-start(bf16[64,12,2048]{2,1,0:T(8,128)(2,1)} %reshape.149), calls=%async_computation.4 | async-start | bytes 8388608 | tf_op jit(solution)/shard_map/all_to_all | solution.py:101
  287.2 7.7 %copy-start.6 = (bf16[768,384]{0,1:T(8,128)(2,1)S(1)}, bf16[768,384]{0,1:T(8,128)(2,1)}, u32[]{:S(2)}) copy-start(bf16[768,384]{0,1:T(8,128)(2,1)} %get-tuple-element.63) | copy-start | bytes 1769476
  335.8 10.2 %copy-start.1 = (bf16[1,4096,384]{2,1,0:T(8,128)(2,1)S(1)}, bf16[1,4096,384]{2,1,0:T(8,128)(2,1)}, u32[]{:S(2)}) copy-start(bf16[1,4096,384]{2,1,0:T(8,128)(2,1)} %param.11) | copy-start | bytes 9437188
Sparse Core Ops, SparseCore 0:
  151.4 33.6 all-gather.1
where the time goes:
time: 360 us; the launch traced here: 353 us
  blocking collectives  94.4 us (26%)
  local copies, waits for them, and re-layouts  68.4 us (19%)
  waiting for transfers between devices  66.4 us (18%)
  matrix products  59.3 us (16%)
  starting transfers between devices  31.9 us (9%)
  other arithmetic  18.1 us (5%)
  between operations  14.3 us (4%)
    all_to_all x1, blocking collectives, body(): lax.all_to_all(send_x.reshape(n_ep, capacity, share), 'ep', split_axis=0,...  61.8 us
    all_to_all x1, waiting for transfers between devices, body(): lax.all_to_all(send_dy.reshape(n_ep, capacity, share), 'ep', split_axis=0...  39.7 us
    all_to_all x1, waiting for transfers between devices, body(): lax.all_to_all(row_grad.reshape(n_ep, capacity, half_width), 'ep', split_...  16.8 us
    all_to_all x1, blocking collectives, body(): lax.all_to_all(send_gate.reshape(n_ep, capacity).astype(jnp.bfloat16), 'e...  16 us
    slice x1, local copies, waits for them, and re-layouts, body(): recv_dy = joined[1]  11.7 us
    all_to_all x1, starting transfers between devices, body(): lax.all_to_all(row_grad.reshape(n_ep, capacity, half_width), 'ep', split_...  10.7 us
    all_to_all x1, starting transfers between devices, body(): lax.all_to_all(send_dy.reshape(n_ep, capacity, share), 'ep', split_axis=0...  10.6 us
    all_to_all x1, starting transfers between devices, body(): lax.all_to_all(gate_total.reshape(n_ep, capacity).astype(jnp.bfloat16), '...  10.5 us
  transfers between devices with their start and end apart: 4, of which 3 were waited for; matrix products, arithmetic and copies ran while one was open for 15% of the time, Pallas kernels for 0%

commit v1 on v0

v1 whole, which is shorter than its diff:
```python
import functools

import jax
import jax.numpy as jnp
from jax import lax
from jax.experimental import pallas as pl
from jax.experimental.pallas import tpu as pltpu
from jax.sharding import PartitionSpec as P

MESH = pl.DeviceIdType.MESH
F32 = jnp.float32
BF16 = jnp.bfloat16
I32 = jnp.int32
CAP = 12
SIDE = 4
CH = 512
NT = (((1,), (1,)), ((), ()))
TN = (((0,), (0,)), ((), ()))
HI = lax.Precision.HIGHEST


def mm(a, b):
    return jnp.dot(a, b, preferred_element_type=F32)


def iota(shape, dim):
    return lax.broadcasted_iota(I32, shape, dim)


def hot(mask):
    return jnp.where(mask, 1.0, 0.0).astype(BF16)


def offsets(p, div, rem):
    q = div(p, 16)
    a = rem(div(p, 8), 2)
    d = rem(div(p, 4), 2)
    oy = rem(p, 4)
    ox = rem(oy + 2 * a + d, 4)
    oz = rem(q + 8 - oy - ox, 4)
    return oz, oy, ox


def scalar_div(a, b):
    return lax.div(a, jnp.int32(b))


def scalar_rem(a, b):
    return lax.rem(a, jnp.int32(b))


def vector_div(a, b):
    return a >> (b.bit_length() - 1)


def vector_rem(a, b):
    return a & (b - 1)


def kernel(
    gs,
    exp_c, exp_r, gat_r, tok, cot, gw, uw, dw,
    gt_o, gg_o, ggw_o, guw_o, gdw_o, sqg_o, squ_o, sqd_o,
    tokv, wgu, wd, send, recv, xv, yv, gp, wt, psend, own, precv, back, gtv, pm, qm,
    gsend, grecv, gps, gpr, rgs, bg, sqs, sqr, sqa,
    d_s, d_r, dg_s, dg_r, f_s, f_r, p_s, p_r, pg_s, pg_r, r_s, r_r, rg_s, rg_r, sq_s, sq_r, ld, st,
):
    n_pos = SIDE ** 3
    ng = n_pos // gs
    wr = 16 * gs
    cr = CAP * gs
    rows_tok, half = tokv.shape[1], tokv.shape[2]
    width = 2 * half
    fold = half - CH
    nk = fold // CH
    ff = wd.shape[0]
    ep = lax.axis_index("ep")
    core = lax.axis_index("tp")
    other = 1 - core
    cz = scalar_div(ep, 16)
    cy = scalar_rem(scalar_div(ep, 4), 4)
    cx = scalar_rem(ep, 4)

    def dest_of(p):
        oz, oy, ox = offsets(p, scalar_div, scalar_rem)
        return (
            scalar_rem(cz + oz, 4) * 16 + scalar_rem(cy + oy, 4) * 4 + scalar_rem(cx + ox, 4)
        )

    def source_of(p):
        oz, oy, ox = offsets(p, scalar_div, scalar_rem)
        return (
            scalar_rem(cz + 4 - oz, 4) * 16
            + scalar_rem(cy + 4 - oy, 4) * 4
            + scalar_rem(cx + 4 - ox, 4)
        )

    def expert_vec(p):
        oz, oy, ox = offsets(p, vector_div, vector_rem)
        return ((cz + oz) & 3) * 16 + ((cy + oy) & 3) * 4 + ((cx + ox) & 3)

    def remote(src, dst, ssem, rsem, ids):
        return pltpu.make_async_remote_copy(
            src_ref=src, dst_ref=dst, send_sem=ssem, recv_sem=rsem,
            device_id=ids, device_id_type=MESH,
        )

    barrier = pltpu.get_barrier_semaphore()

    def greet(p, carry):
        pl.semaphore_signal(
            barrier, inc=1, device_id={"ep": dest_of(p)}, device_id_type=MESH
        )
        return carry

    lax.fori_loop(1, n_pos, greet, 0)
    pl.semaphore_signal(barrier, inc=1, device_id={"tp": other}, device_id_type=MESH)
    mine = pl.ds(pl.multiple_of(core * half, half), half)
    loads = [
        pltpu.make_async_copy(tok.at[:, mine], tokv.at[0], ld.at[0]),
        pltpu.make_async_copy(cot.at[:, mine], tokv.at[1], ld.at[1]),
        pltpu.make_async_copy(gw, wgu.at[:, 0:ff], ld.at[2]),
        pltpu.make_async_copy(uw, wgu.at[:, ff : 2 * ff], ld.at[3]),
        pltpu.make_async_copy(dw, wd, ld.at[4]),
    ]
    for copy in loads:
        copy.start()

    e_lane = [exp_r[j : j + 1, :] for j in range(2)]
    e_sub = [exp_c[:, j : j + 1] for j in range(2)]
    hot_t = [
        jnp.where(iota((n_pos, rows_tok), 0) == e_lane[j], 1.0, 0.0).astype(F32) for j in range(2)
    ]
    hot_c = [
        jnp.where(iota((rows_tok, n_pos), 1) == e_sub[j], 1.0, 0.0).astype(F32) for j in range(2)
    ]
    upper = hot(iota((rows_tok, rows_tok), 0) < iota((rows_tok, rows_tok), 1))
    lower = hot(iota((rows_tok, rows_tok), 1) < iota((rows_tok, rows_tok), 0))
    prior_t = mm((hot_t[0] + hot_t[1]).astype(BF16), upper)
    prior_c = mm(lower, (hot_c[0] + hot_c[1]).astype(BF16))
    slot_lane = [
        jnp.sum(hot_t[j] * prior_t, axis=0, keepdims=True).astype(I32) for j in range(2)
    ]
    slot_sub = [
        jnp.sum(hot_c[j] * prior_c, axis=1, keepdims=True).astype(I32) for j in range(2)
    ]
    key_lane = [e_lane[j] * 16 + slot_lane[j] for j in range(2)]
    key_sub = [e_sub[j] * 16 + slot_sub[j] for j in range(2)]

    place = expert_vec(iota((n_pos, rows_tok), 0))
    gate_rows = jnp.zeros((n_pos, 128), F32)
    for j in range(2):
        picked = jnp.where(place == e_lane[j], gat_r[j : j + 1, :], 0.0)
        slots = jnp.where(iota((rows_tok, 128), 1) == slot_sub[j], 1.0, 0.0)
        gate_rows += jnp.dot(picked, slots, preferred_element_type=F32, precision=HI)
    gsend[...] = gate_rows.reshape(n_pos, 1, 128)

    to_c, of_w = iota((cr, wr), 0), iota((cr, wr), 1)
    wire_r, wire_s = of_w & 15, of_w >> 4
    pm[0] = hot((wire_r < CAP) & (to_c == CAP * wire_s + wire_r))
    for k in range(nk):
        pm[1 + k] = hot((wire_r >= CAP) & (to_c == CAP * wire_s + 4 * k + wire_r - CAP))
    of_w, to_c = iota((wr, cr), 0), iota((wr, cr), 1)
    wire_r, wire_s = of_w & 15, of_w >> 4
    qm[0] = hot((wire_r < CAP) & (to_c == CAP * wire_s + wire_r))
    for k in range(nk):
        qm[1 + k] = hot((wire_r >= CAP) & (to_c == CAP * wire_s + 4 * k + wire_r - CAP))

    loads[0].wait()
    loads[1].wait()

    def wire_rows(g):
        return pl.ds(pl.multiple_of(g * wr, wr), wr)

    def block_rows(p):
        return pl.ds(pl.multiple_of(p * 16, 16), 16)

    def dispatch(g, carry):
        row = iota((wr, rows_tok), 0)
        r = row & 15
        base = expert_vec(g * gs + (row >> 4)) * 16
        direct = base + r
        folded = jnp.where(r >= CAP, base + r - CAP, -4096)
        s_dir = hot((key_lane[0] == direct) | (key_lane[1] == direct))
        s_fold = [
            hot((key_lane[0] == folded + 4 * k) | (key_lane[1] == folded + 4 * k))
            for k in range(nk)
        ]
        for a in range(2):
            last = tokv[a, :, fold : fold + CH]
            for k in range(nk):
                part = mm(s_dir, tokv[a, :, k * CH : (k + 1) * CH]) + mm(s_fold[k], last)
                send[wire_rows(g), a * fold + k * CH : a * fold + (k + 1) * CH] = part.astype(BF16)

        @pl.when(g == 0)
        def _():
            pl.semaphore_wait(barrier, n_pos)
            recv[core, 0:16, :] = send[0:16, :]
            grecv[0] = gsend[0]

        def start(i, carry):
            p = g * gs + i

            @pl.when(p > 0)
            def _():
                dest = {"ep": dest_of(p)}
                remote(
                    gsend.at[p], grecv.at[p], dg_s.at[g], dg_r.at[g], dest
                ).start()
                remote(
                    send.at[block_rows(p)], recv.at[core, block_rows(p)],
                    d_s.at[g], d_r.at[g], dest,
                ).start()

            return carry

        lax.fori_loop(0, gs, start, 0)
        return carry

    lax.fori_loop(0, ng, dispatch, 0)
    for copy in loads[2:]:
        copy.wait()

    def group_wait(g, make, recv_side):
        @pl.when(g == 0)
        def _():
            copy = make(1, gs - 1)
            copy.wait_recv() if recv_side else copy.wait_send()

        @pl.when(g > 0)
        def _():
            copy = make(g * gs, gs)
            copy.wait_recv() if recv_side else copy.wait_send()

    partner = {"tp": other}

    def d_copy(g):
        return lambda p, n: remote(
            send.at[pl.ds(pl.multiple_of(p * 16, 16), n * 16)],
            recv.at[core, pl.ds(pl.multiple_of(p * 16, 16), n * 16)],
            d_s.at[g], d_r.at[g], partner,
        )

    def dg_copy(g):
        return lambda p, n: remote(
            gsend.at[pl.ds(p, n)], grecv.at[pl.ds(p, n)], dg_s.at[g], dg_r.at[g], partner
        )

    def r_copy(g):
        return lambda p, n: remote(
            send.at[pl.ds(pl.multiple_of(p * 16, 16), n * 16), 0:fold],
            back.at[pl.ds(pl.multiple_of(p * 16, 16), n * 16)],
            r_s.at[g], r_r.at[g], partner,
        )

    def rg_copy(g):
        return lambda p, n: remote(
            rgs.at[pl.ds(p, n)], bg.at[pl.ds(p, n)], rg_s.at[g], rg_r.at[g], partner
        )

    def expert(g, carry):
        rows_w = wire_rows(g)
        rows_c = pl.ds(pl.multiple_of(g * cr, cr), cr)
        group_wait(g, d_copy(g), True)
        forward = remote(
            recv.at[core, rows_w], recv.at[core, rows_w], f_s, f_r.at[g], partner
        )
        forward.start()
        group_wait(g, dg_copy(g), True)

        def unfold(h):
            for a, into in ((0, xv), (1, yv)):
                tail = jnp.zeros((cr, CH), F32)
                for k in range(nk):
                    piece = recv[h, rows_w, a * fold + k * CH : a * fold + (k + 1) * CH]
                    at = pl.ds(pl.multiple_of(h * half + k * CH, CH), CH)
                    into[rows_c, at] = mm(pm[0], piece).astype(BF16)
                    tail += mm(pm[1 + k], piece)
                at = pl.ds(pl.multiple_of(h * half + fold, CH), CH)
                into[rows_c, at] = tail.astype(BF16)

        unfold(core)
        diff = iota((cr, gs), 0) - CAP * iota((cr, gs), 1)
        inside = (diff >= 0) & (diff < CAP)
        row_src = jnp.where(inside, 1.0, 0.0)
        row_slot = jnp.sum(jnp.where(inside, diff, 0), axis=1, keepdims=True)
        slot_mask = iota((cr, 128), 1) == row_slot
        gate_block = grecv[pl.ds(g * gs, gs)].reshape(gs, 128)
        spread = jnp.dot(row_src, gate_block, preferred_element_type=F32, precision=HI)
        gate = jnp.sum(jnp.where(slot_mask, spread, 0.0), axis=1, keepdims=True)
        forward.wait()
        unfold(other)

        pre = mm(xv[rows_c, :], wgu[...])
        hid_grad = lax.dot_general(yv[rows_c, :], wd[...], NT, preferred_element_type=F32)
        pre_gate, pre_up = pre[:, :ff], pre[:, ff:]
        sig = jax.nn.sigmoid(pre_gate)
        silu = pre_gate * sig
        hidden = (silu * pre_up).astype(BF16).astype(F32)
        gate_part = jnp.sum(hidden * hid_grad, axis=1, keepdims=True)
        scaled = gate * hid_grad
        gp[rows_c, 0:ff] = (scaled * pre_up * sig * (1.0 + pre_gate * (1.0 - sig))).astype(BF16)
        gp[rows_c, ff : 2 * ff] = (scaled * silu).astype(BF16)
        wt[rows_c, :] = (gate * hidden).astype(BF16)
        grads = gp[rows_c, :]
        theirs = wgu[pl.ds(pl.multiple_of(other * half, half), half), :]
        psend[...] = lax.dot_general(grads, theirs, NT, preferred_element_type=F32).astype(BF16)
        gps[...] = lax.dot_general(
            row_src, jnp.where(slot_mask, gate_part, 0.0), TN,
            preferred_element_type=F32, precision=HI,
        )
        swap = remote(psend, precv.at[g], p_s, p_r.at[g], partner)
        swap_gate = remote(gps, gpr.at[g], pg_s, pg_r.at[g], partner)
        swap.start()
        swap_gate.start()
        ours = wgu[pl.ds(pl.multiple_of(core * half, half), half), :]
        own[...] = lax.dot_general(grads, ours, NT, preferred_element_type=F32).astype(BF16)
        group_wait(g, d_copy(g), False)
        swap.wait()
        swap_gate.wait()

        def row_grad(k):
            cols = slice(k * CH, (k + 1) * CH)
            return (own[:, cols].astype(F32) + precv[g, :, cols].astype(F32)).astype(BF16)

        tail = row_grad(nk)
        for k in range(nk):
            part = mm(qm[0], row_grad(k)) + mm(qm[1 + k], tail)
            send[rows_w, k * CH : (k + 1) * CH] = part.astype(BF16)
        rgs[pl.ds(g * gs, gs)] = (gps[...] + gpr[g]).reshape(gs, 1, 128)

        @pl.when(g == 0)
        def _():
            back[0:16, :] = send[0:16, 0:fold]
            bg[0] = rgs[0]

        def start(i, carry):
            p = g * gs + i

            @pl.when(p > 0)
            def _():
                source = {"ep": source_of(p)}
                remote(rgs.at[p], bg.at[p], rg_s.at[g], rg_r.at[g], source).start()
                remote(
                    send.at[block_rows(p), 0:fold], back.at[block_rows(p)],
                    r_s.at[g], r_r.at[g], source,
                ).start()

            return carry

        lax.fori_loop(0, gs, start, 0)
        return carry

    lax.fori_loop(0, ng, expert, 0)

    def grad_gu(i, carry):
        cols = pl.ds(pl.multiple_of(i * CH, CH), CH)
        g = lax.dot_general(xv[:, cols], gp[...], TN, preferred_element_type=F32).astype(BF16)
        wgu[cols, :] = g
        sq = g.astype(F32)
        sq = sq * sq
        ones = jnp.ones((8, ff), F32)
        sqs[0:8, cols] = lax.dot_general(ones, sq[:, :ff], NT, preferred_element_type=F32)
        sqs[8:16, cols] = lax.dot_general(ones, sq[:, ff:], NT, preferred_element_type=F32)
        pltpu.make_async_copy(wgu.at[cols, 0:ff], ggw_o.at[cols, :], st.at[0]).start()
        pltpu.make_async_copy(wgu.at[cols, ff : 2 * ff], guw_o.at[cols, :], st.at[1]).start()
        return carry

    lax.fori_loop(0, width // CH, grad_gu, 0)
    sums = remote(sqs, sqr, sq_s, sq_r, partner)
    sums.start()
    sqa[...] = jnp.zeros_like(sqa)

    def grad_d(i, carry):
        cols = pl.ds(pl.multiple_of(i * CH, CH), CH)
        g = lax.dot_general(wt[...], yv[:, cols], TN, preferred_element_type=F32).astype(BF16)
        wd[:, cols] = g
        sq = g.astype(F32)
        sq = sq * sq
        acc = sq[:, 0:128]
        for k in range(1, CH // 128):
            acc += sq[:, k * 128 : (k + 1) * 128]
        sqa[...] += acc
        pltpu.make_async_copy(wd.at[:, cols], gdw_o.at[:, cols], st.at[2]).start()
        return carry

    lax.fori_loop(0, width // CH, grad_d, 0)
    sq_down = lax.dot_general(
        jnp.ones((8, 128), F32), sqa[...], NT, preferred_element_type=F32, precision=HI
    )
    sqd_o[...] = sq_down[0:1, :] * (1.0 / width)

    lane = iota((rows_tok, 16 * n_pos), 1)
    r = lane & 15
    base = expert_vec(lane >> 4) * 16
    direct = base + r
    folded = jnp.where(r >= CAP, base + r - CAP, -4096)
    homes = [(key_sub[0] == direct) | (key_sub[1] == direct)] + [
        (key_sub[0] == folded + 4 * k) | (key_sub[1] == folded + 4 * k) for k in range(nk)
    ]
    n_wire = 16 * n_pos
    for m in range(nk + 1):
        tokv[m // 2, :, (m % 2) * n_wire : (m % 2 + 1) * n_wire] = hot(homes[m])

    def home(m):
        return tokv[m // 2, :, (m % 2) * n_wire : (m % 2 + 1) * n_wire]

    sums.wait()
    scale = 1.0 / (2 * ff)
    sqg_o[...] = (sqs[0:1, :] + sqr[0:1, :]) * scale
    squ_o[...] = (sqs[8:9, :] + sqr[8:9, :]) * scale

    def arrive(g, carry):
        group_wait(g, rg_copy(g), True)
        group_wait(g, r_copy(g), True)
        return carry

    lax.fori_loop(0, ng, arrive, 0)
    tail = jnp.zeros((rows_tok, CH), F32)
    for k in range(nk):
        piece = back[:, k * CH : (k + 1) * CH]
        gtv[:, k * CH : (k + 1) * CH] = mm(home(0), piece).astype(BF16)
        tail += mm(home(1 + k), piece)
    gtv[:, fold : fold + CH] = tail.astype(BF16)
    out = pltpu.make_async_copy(gtv, gt_o, ld.at[0])
    out.start()
    back_gate = bg[...].reshape(n_pos, 128)
    place = expert_vec(iota((rows_tok, n_pos), 1))
    picked = []
    for j in range(2):
        rows = jnp.dot(
            jnp.where(place == e_sub[j], 1.0, 0.0), back_gate,
            preferred_element_type=F32, precision=HI,
        )
        picked.append(
            jnp.sum(
                jnp.where(iota((rows_tok, 128), 1) == slot_sub[j], rows, 0.0),
                axis=1, keepdims=True,
            )
        )
    gg_o[...] = jnp.where(iota((rows_tok, 2), 1) == 0, picked[0], picked[1])

    def drain(g, carry):
        group_wait(g, dg_copy(g), False)
        group_wait(g, rg_copy(g), False)
        group_wait(g, r_copy(g), False)
        return carry

    lax.fori_loop(0, ng, drain, 0)
    pltpu.make_async_copy(wgu.at[:, 0:ff], ggw_o, st.at[0]).wait()
    pltpu.make_async_copy(wgu.at[:, ff : 2 * ff], guw_o, st.at[1]).wait()
    pltpu.make_async_copy(wd, gdw_o, st.at[2]).wait()
    out.wait()


GS = 16


def body(tokens, cotangent, gates, experts, gate_w, up_w, down_w):
    rows, width = tokens.shape
    half = width // 2
    ff = down_w.shape[1]
    n_pos = SIDE ** 3
    ng = n_pos // GS
    n_wire = 16 * n_pos
    n_rows = CAP * n_pos
    fold = half - CH
    wr, cr = 16 * GS, CAP * GS
    any_spec = pl.BlockSpec(memory_space=pl.ANY)
    vmem = pl.BlockSpec(memory_space=pltpu.VMEM)
    dma = pltpu.SemaphoreType.DMA
    outs = pl.pallas_call(
        functools.partial(kernel, GS),
        out_shape=(
            jax.ShapeDtypeStruct((rows, half), BF16),
            jax.ShapeDtypeStruct((rows, 2), F32),
            jax.ShapeDtypeStruct((width, ff), BF16),
            jax.ShapeDtypeStruct((width, ff), BF16),
            jax.ShapeDtypeStruct((ff, width), BF16),
            jax.ShapeDtypeStruct((1, width), F32),
            jax.ShapeDtypeStruct((1, width), F32),
            jax.ShapeDtypeStruct((1, ff), F32),
        ),
        in_specs=[vmem, vmem, vmem] + [any_spec] * 5,
        out_specs=(any_spec, vmem, any_spec, any_spec, any_spec, vmem, vmem, vmem),
        scratch_shapes=[
            pltpu.VMEM((2, rows, half), BF16),
            pltpu.VMEM((width, 2 * ff), BF16),
            pltpu.VMEM((ff, width), BF16),
            pltpu.VMEM((n_wire, 2 * fold), BF16),
            pltpu.VMEM((2, n_wire, 2 * fold), BF16),
            pltpu.VMEM((n_rows, width), BF16),
            pltpu.VMEM((n_rows, width), BF16),
            pltpu.VMEM((n_rows, 2 * ff), BF16),
            pltpu.VMEM((n_rows, ff), BF16),
            pltpu.VMEM((cr, half), BF16),
            pltpu.VMEM((cr, half), BF16),
            pltpu.VMEM((ng, cr, half), BF16),
            pltpu.VMEM((n_wire, fold), BF16),
            pltpu.VMEM((rows, half), BF16),
            pltpu.VMEM((4, cr, wr), BF16),
            pltpu.VMEM((4, wr, cr), BF16),
            pltpu.VMEM((n_pos, 1, 128), F32),
            pltpu.VMEM((n_pos, 1, 128), F32),
            pltpu.VMEM((GS, 128), F32),
            pltpu.VMEM((ng, GS, 128), F32),
            pltpu.VMEM((n_pos, 1, 128), F32),
            pltpu.VMEM((n_pos, 1, 128), F32),
            pltpu.VMEM((16, width), F32),
            pltpu.VMEM((16, width), F32),
            pltpu.VMEM((ff, 128), F32),
            dma((ng,)), dma((ng,)), dma((ng,)), dma((ng,)),
            dma, dma((ng,)), dma, dma((ng,)), dma, dma((ng,)),
            dma((ng,)), dma((ng,)), dma((ng,)), dma((ng,)),
            dma, dma, dma((5,)), dma((3,)),
        ],
        compiler_params=pltpu.CompilerParams(
            collective_id=0, has_side_effects=True, vmem_limit_bytes=67043328
        ),
    )(experts, experts.T, gates.T, tokens, cotangent, gate_w[0], up_w[0], down_w[0])
    gt, gg, ggw, guw, gdw, sqg, squ, sqd = outs
    return gt, gg, ggw[None], guw[None], gdw[None], sqg, squ, sqd


def solution(mesh):
    placed = (
        P("ep", None),
        P("ep", None),
        P("ep", None),
        P("ep", None),
        P("ep", None, "tp"),
        P("ep", None, "tp"),
        P("ep", "tp", None),
    )
    return jax.shard_map(
        body,
        mesh=mesh,
        in_specs=placed,
        out_specs=(
            P("ep", "tp"),
            P("ep", None),
            P("ep", None, "tp"),
            P("ep", None, "tp"),
            P("ep", "tp", None),
            P("ep", None),
            P("ep", None),
            P("ep", "tp"),
        ),
        check_vma=False,
    )
```

time: 360 us -> 162 us (0.45)
  the two profiles are of different devices: /device:TPU:88 before, /device:TPU:43 now
where the time goes in v1:
time: 162 us; the launch traced here: 161 us
  Pallas kernels  145 us (90%)
  local copies, waits for them, and re-layouts  15.8 us (10%)
    pallas_call x1, Pallas kernels, body(): pl.pallas_call(functools.partial(kernel, GS), out_shape=(jax.ShapeDtypeSt...  145 us
    unnamed x19, local copies, waits for them, and re-layouts  15.8 us

profile of v1, /device:TPU:43, one launch (start us, length us, event | category | flops | bytes accessed | tf_op | source)
XLA Modules:
  0.0 161.3 jit_solution(15703124895371081903)
XLA Ops:
  0.6 1.5 copy.15.exp_c
  2.1 144.8 %shard_map.134 = (bf16[256,2048]{1,0:T(8,128)(2,1)}, f32[256,2]{1,0:T(8,128)}, bf16[4096,384]{1,0:T(8,128)(2,1)}, bf16[4096,384]{1,0:T(8,128)(2,1)}, bf16[384,40...) custom-call(s32[256,2]{1,0:T(8,128)} %copy.15.exp_c, s32[2,256]{1,0:T(2,128)} %bitcast.14, ...), custom_call_target="tpu_custom_call" | custom-call | tf_op jit(solution)/shard_map/pallas_call | solution.py:472
  147.0 1.6 copy.16
  148.5 2.3 %copy.24 = bf16[256,2048]{1,0:T(8,128)(2,1)} copy(bf16[256,2048]{1,0:T(8,128)(2,1)} %get-tuple-element.40) | data formatting | bytes 2097152
  150.8 0.0 copy-start.1
  150.8 4.0 %copy.25 = bf16[1,4096,384]{2,1,0:T(8,128)(2,1)} copy(bf16[1,4096,384]{2,1,0:T(8,128)(2,1)} %bitcast.10) | data formatting | bytes 6291456
  154.8 0.0 copy-done.1
  154.8 0.0 copy-start
  154.8 1.7 %copy.26 = bf16[1,4096,384]{2,1,0:T(8,128)(2,1)} copy(bf16[1,4096,384]{2,1,0:T(8,128)(2,1)S(1)} %bitcast.9) | data formatting | bytes 6291456
  156.5 1.4 copy-done
  157.9 0.0 copy-start.3
  157.9 0.0 copy-start.2
  157.9 0.0 copy-start.4
  157.9 1.7 %copy.27 = bf16[1,384,4096]{2,1,0:T(8,128)(2,1)} copy(bf16[1,384,4096]{2,1,0:T(8,128)(2,1)S(1)} %bitcast.8) | data formatting | bytes 6291456
  159.5 0.0 copy-done.3
  159.5 0.6 copy.28
  160.1 0.0 copy-done.2
  160.2 0.6 copy.29
  160.8 0.0 copy-done.4
  160.8 0.6 copy.30
Async XLA Ops:
  150.8 4.0 %copy-start.1 = (bf16[4096,384]{1,0:T(8,128)(2,1)S(1)}, bf16[4096,384]{1,0:T(8,128)(2,1)}, u32[]{:S(2)}) copy-start(bf16[4096,384]{1,0:T(8,128)(2,1)} %get-tuple-element.19) | copy-start | bytes 9437188
  154.8 3.0 %copy-start = (bf16[384,4096]{1,0:T(8,128)(2,1)S(1)}, bf16[384,4096]{1,0:T(8,128)(2,1)}, u32[]{:S(2)}) copy-start(bf16[384,4096]{1,0:T(8,128)(2,1)} %get-tuple-element.20) | copy-start | bytes 9437188
  157.9 1.7 %copy-start.3 = (f32[1,4096]{1,0:T(1,128)S(1)}, f32[1,4096]{1,0:T(1,128)}, u32[]{:S(2)}) copy-start(f32[1,4096]{1,0:T(1,128)} %get-tuple-element.45) | copy-start | bytes 49156
  157.9 2.3 %copy-start.2 = (f32[1,4096]{1,0:T(1,128)S(1)}, f32[1,4096]{1,0:T(1,128)}, u32[]{:S(2)}) copy-start(f32[1,4096]{1,0:T(1,128)} %get-tuple-element.46) | copy-start | bytes 49156
  157.9 2.9 %copy-start.4 = (f32[1,384]{1,0:T(1,128)S(1)}, f32[1,384]{1,0:T(1,128)}, u32[]{:S(2)}) copy-start(f32[1,384]{1,0:T(1,128)} %get-tuple-element.47) | copy-start | bytes 4612

commit v2 on v1

v2 whole, which is shorter than its diff:
```python
import functools

import jax
import jax.numpy as jnp
from jax import lax
from jax.experimental import pallas as pl
from jax.experimental.pallas import tpu as pltpu
from jax.sharding import PartitionSpec as P

MESH = pl.DeviceIdType.MESH
F32 = jnp.float32
BF16 = jnp.bfloat16
I32 = jnp.int32
CAP = 12
SIDE = 4
CH = 512
NT = (((1,), (1,)), ((), ()))
TN = (((0,), (0,)), ((), ()))
HI = lax.Precision.HIGHEST


def mm(a, b):
    return jnp.dot(a, b, preferred_element_type=F32)


def iota(shape, dim):
    return lax.broadcasted_iota(I32, shape, dim)


def hot(mask):
    return jnp.where(mask, 1.0, 0.0).astype(BF16)


def offsets(p, div, rem):
    q = div(p, 16)
    a = rem(div(p, 8), 2)
    d = rem(div(p, 4), 2)
    oy = rem(p, 4)
    ox = rem(oy + 2 * a + d, 4)
    oz = rem(q + 8 - oy - ox, 4)
    return oz, oy, ox


def scalar_div(a, b):
    return lax.div(a, jnp.int32(b))


def scalar_rem(a, b):
    return lax.rem(a, jnp.int32(b))


def vector_div(a, b):
    return a >> (b.bit_length() - 1)


def vector_rem(a, b):
    return a & (b - 1)


def kernel(
    gs,
    exp_r, gat_r, tok, cot, gw, uw, dw,
    wgu, wd, sqg_o, squ_o, sqd_o, back, bg, tokv, slot_o, place_o,
    send, recv, xv, yv, gp, wt, psend, own, precv, pm, qm,
    gsend, grecv, gps, gpr, rgs, sqs, sqr, sqa,
    d_s, d_r, dg_s, dg_r, f_s, f_r, p_s, p_r, pg_s, pg_r, r_s, r_r, rg_s, rg_r, sq_s, sq_r, ld,
):
    n_pos = SIDE ** 3
    ng = n_pos // gs
    wr = 16 * gs
    cr = CAP * gs
    rows_tok, half = tokv.shape[1], tokv.shape[2]
    width = 2 * half
    fold = half - CH
    nk = fold // CH
    ff = wd.shape[0]
    ep = lax.axis_index("ep")
    core = lax.axis_index("tp")
    other = 1 - core
    cz = scalar_div(ep, 16)
    cy = scalar_rem(scalar_div(ep, 4), 4)
    cx = scalar_rem(ep, 4)

    def offset_at(i):
        oy = i % 4
        return oy, (oy + 2 * (i // 8) + (i // 4) % 2) % 4

    ys = [scalar_rem(cy + o, 4) * 4 for o in range(4)]
    xs = [scalar_rem(cx + o, 4) for o in range(4)]

    def dest_of(g, i):
        oy, ox = offset_at(i)
        return scalar_rem(cz + g + 8 - oy - ox, 4) * 16 + ys[oy] + xs[ox]

    def source_of(g, i):
        oy, ox = offset_at(i)
        return scalar_rem(cz + 4 - g + oy + ox, 4) * 16 + ys[-oy % 4] + xs[-ox % 4]

    def each_peer(g, act):
        for i in range(gs):
            if i == 0:
                pl.when(g > 0)(functools.partial(act, 0))
            else:
                act(i)

    def expert_vec(p):
        oz, oy, ox = offsets(p, vector_div, vector_rem)
        return ((cz + oz) & 3) * 16 + ((cy + oy) & 3) * 4 + ((cx + ox) & 3)

    def remote(src, dst, ssem, rsem, ids):
        return pltpu.make_async_remote_copy(
            src_ref=src, dst_ref=dst, send_sem=ssem, recv_sem=rsem,
            device_id=ids, device_id_type=MESH,
        )

    mine = pl.ds(pl.multiple_of(core * half, half), half)
    loads = [
        pltpu.make_async_copy(tok.at[:, mine], tokv.at[0], ld.at[0]),
        pltpu.make_async_copy(cot.at[:, mine], tokv.at[1], ld.at[1]),
        pltpu.make_async_copy(gw, wgu.at[:, 0:ff], ld.at[2]),
        pltpu.make_async_copy(uw, wgu.at[:, ff : 2 * ff], ld.at[3]),
        pltpu.make_async_copy(dw, wd, ld.at[4]),
    ]
    for copy in loads[:2]:
        copy.start()
    barrier = pltpu.get_barrier_semaphore()

    def greet(g, carry):
        def one(i):
            pl.semaphore_signal(
                barrier, inc=1, device_id={"ep": dest_of(g, i)}, device_id_type=MESH
            )

        each_peer(g, one)
        return carry

    lax.fori_loop(0, ng, greet, 0)
    pl.semaphore_signal(barrier, inc=1, device_id={"tp": other}, device_id_type=MESH)
    e_lane = [exp_r[j : j + 1, :] for j in range(2)]
    hot_t = [
        jnp.where(iota((n_pos, rows_tok), 0) == e_lane[j], 1.0, 0.0).astype(F32) for j in range(2)
    ]
    upper = hot(iota((rows_tok, rows_tok), 0) < iota((rows_tok, rows_tok), 1))
    prior_t = mm((hot_t[0] + hot_t[1]).astype(BF16), upper)
    slot_lane = [
        jnp.sum(hot_t[j] * prior_t, axis=0, keepdims=True).astype(I32) for j in range(2)
    ]
    key_lane = [e_lane[j] * 16 + slot_lane[j] for j in range(2)]
    for j in range(2):
        slot_o[j : j + 1, :] = slot_lane[j]

    place = expert_vec(iota((n_pos, rows_tok), 0))
    gate_rows = jnp.zeros((n_pos, 128), F32)
    for j in range(2):
        place_o[j] = jnp.where(place == e_lane[j], 1.0, 0.0)
        picked = place_o[j] * gat_r[j : j + 1, :]
        slots = jnp.where(iota((128, rows_tok), 0) == slot_lane[j], 1.0, 0.0)
        gate_rows += lax.dot_general(
            picked, slots, NT, preferred_element_type=F32, precision=HI
        )
    gsend[...] = gate_rows.reshape(n_pos, 1, 128)

    loads[0].wait()
    loads[1].wait()
    for copy in loads[2:]:
        copy.start()

    def wire_rows(g):
        return pl.ds(pl.multiple_of(g * wr, wr), wr)

    def block_rows(g, i):
        return pl.ds(pl.multiple_of(g * wr + i * 16, 16), 16)

    def block(g, i, a, dest):
        rows, cols = block_rows(g, i), slice(a * fold, (a + 1) * fold)
        return remote(
            send.at[rows, cols], recv.at[core, rows, cols],
            d_s.at[2 * g + a], d_r.at[2 * g + a], dest,
        )

    def dispatch(g, carry):
        row = iota((wr, rows_tok), 0)
        r = row & 15
        base = expert_vec(g * gs + (row >> 4)) * 16
        direct = base + r
        folded = jnp.where(r >= CAP, base + r - CAP, -4096)
        s_dir = hot((key_lane[0] == direct) | (key_lane[1] == direct))
        s_fold = [
            hot((key_lane[0] == folded + 4 * k) | (key_lane[1] == folded + 4 * k))
            for k in range(nk)
        ]
        for a in range(2):
            last = tokv[a, :, fold : fold + CH]
            for k in range(nk):
                part = mm(s_dir, tokv[a, :, k * CH : (k + 1) * CH]) + mm(s_fold[k], last)
                send[wire_rows(g), a * fold + k * CH : a * fold + (k + 1) * CH] = part.astype(BF16)

        @pl.when(g == 0)
        def _():
            pl.semaphore_wait(barrier, n_pos)
            recv[core, 0:16, :] = send[0:16, :]
            grecv[0] = gsend[0]

        def start(i):
            dest = {"ep": dest_of(g, i)}
            p = g * gs + i
            remote(gsend.at[p], grecv.at[p], dg_s.at[g], dg_r.at[g], dest).start()
            block(g, i, 0, dest).start()

        def start_second(i):
            block(g, i, 1, {"ep": dest_of(g, i)}).start()

        each_peer(g, start)
        each_peer(g, start_second)
        return carry

    lax.fori_loop(0, ng, dispatch, 0)

    to_c, of_w = iota((cr, wr), 0), iota((cr, wr), 1)
    wire_r, wire_s = of_w & 15, of_w >> 4
    pm[0] = hot((wire_r < CAP) & (to_c == CAP * wire_s + wire_r))
    for k in range(nk):
        pm[1 + k] = hot((wire_r >= CAP) & (to_c == CAP * wire_s + 4 * k + wire_r - CAP))
    of_w, to_c = iota((wr, cr), 0), iota((wr, cr), 1)
    wire_r, wire_s = of_w & 15, of_w >> 4
    qm[0] = hot((wire_r < CAP) & (to_c == CAP * wire_s + wire_r))
    for k in range(nk):
        qm[1 + k] = hot((wire_r >= CAP) & (to_c == CAP * wire_s + 4 * k + wire_r - CAP))

    for copy in loads[2:]:
        copy.wait()

    def group_wait(g, make, recv_side):
        @pl.when(g == 0)
        def _():
            copy = make(1, gs - 1)
            copy.wait_recv() if recv_side else copy.wait_send()

        @pl.when(g > 0)
        def _():
            copy = make(g * gs, gs)
            copy.wait_recv() if recv_side else copy.wait_send()

    partner = {"tp": other}

    def d_copy(g, a):
        cols = slice(a * fold, (a + 1) * fold)
        return lambda p, n: remote(
            send.at[pl.ds(pl.multiple_of(p * 16, 16), n * 16), cols],
            recv.at[core, pl.ds(pl.multiple_of(p * 16, 16), n * 16), cols],
            d_s.at[2 * g + a], d_r.at[2 * g + a], partner,
        )

    def dg_copy(g):
        return lambda p, n: remote(
            gsend.at[pl.ds(p, n)], grecv.at[pl.ds(p, n)], dg_s.at[g], dg_r.at[g], partner
        )

    def r_copy(g):
        return lambda p, n: remote(
            send.at[pl.ds(pl.multiple_of(p * 16, 16), n * 16), 0:fold],
            back.at[pl.ds(pl.multiple_of(p * 16, 16), n * 16)],
            r_s.at[g], r_r.at[g], partner,
        )

    def rg_copy(g):
        return lambda p, n: remote(
            rgs.at[pl.ds(p, n)], bg.at[pl.ds(p, n)], rg_s.at[g], rg_r.at[g], partner
        )

    def send_back(g):
        def start(i):
            source = {"ep": source_of(g, i)}
            p = g * gs + i
            remote(rgs.at[p], bg.at[p], rg_s.at[g], rg_r.at[g], source).start()
            remote(
                send.at[block_rows(g, i), 0:fold], back.at[block_rows(g, i)],
                r_s.at[g], r_r.at[g], source,
            ).start()

        each_peer(g, start)

    def expert(g, carry):
        rows_w = wire_rows(g)
        rows_c = pl.ds(pl.multiple_of(g * cr, cr), cr)

        def forward(a):
            cols = slice(a * fold, (a + 1) * fold)
            return remote(
                recv.at[core, rows_w, cols], recv.at[core, rows_w, cols],
                f_s.at[a], f_r.at[2 * g + a], partner,
            )

        def unfold(h, a):
            into = (xv, yv)[a]
            tail = jnp.zeros((cr, CH), F32)
            for k in range(nk):
                piece = recv[h, rows_w, a * fold + k * CH : a * fold + (k + 1) * CH]
                at = pl.ds(pl.multiple_of(h * half + k * CH, CH), CH)
                into[rows_c, at] = mm(pm[0], piece).astype(BF16)
                tail += mm(pm[1 + k], piece)
            at = pl.ds(pl.multiple_of(h * half + fold, CH), CH)
            into[rows_c, at] = tail.astype(BF16)

        def half_of(h):
            return pl.ds(pl.multiple_of(h * half, half), half)

        def pre_half(h):
            return mm(xv[rows_c, half_of(h)], wgu[half_of(h), :])

        def hid_half(h):
            return lax.dot_general(
                yv[rows_c, half_of(h)], wd[:, half_of(h)], NT, preferred_element_type=F32
            )

        group_wait(g, d_copy(g, 0), True)
        forward(0).start()
        unfold(core, 0)
        group_wait(g, d_copy(g, 1), True)
        forward(1).start()
        for at, due in RETURNS:
            @pl.when(g == at)
            def _():
                for other_g in due:
                    send_back(jnp.int32(other_g))

        pre_own = pre_half(core)
        unfold(core, 1)
        hid_own = hid_half(core)
        group_wait(g, dg_copy(g), True)
        diff = iota((cr, gs), 0) - CAP * iota((cr, gs), 1)
        inside = (diff >= 0) & (diff < CAP)
        row_src = jnp.where(inside, 1.0, 0.0)
        row_slot = jnp.sum(jnp.where(inside, diff, 0), axis=1, keepdims=True)
        slot_mask = iota((cr, 128), 1) == row_slot
        gate_block = grecv[pl.ds(g * gs, gs)].reshape(gs, 128)
        spread = jnp.dot(row_src, gate_block, preferred_element_type=F32, precision=HI)
        gate = jnp.sum(jnp.where(slot_mask, spread, 0.0), axis=1, keepdims=True)
        forward(0).wait()
        unfold(other, 0)
        pre = pre_own + pre_half(other)
        forward(1).wait()
        unfold(other, 1)
        hid_grad = hid_own + hid_half(other)
        pre_gate, pre_up = pre[:, :ff], pre[:, ff:]
        sig = jax.nn.sigmoid(pre_gate)
        silu = pre_gate * sig
        hidden = (silu * pre_up).astype(BF16).astype(F32)
        gate_part = jnp.sum(hidden * hid_grad, axis=1, keepdims=True)
        scaled = gate * hid_grad
        gp[rows_c, 0:ff] = (scaled * pre_up * sig * (1.0 + pre_gate * (1.0 - sig))).astype(BF16)
        gp[rows_c, ff : 2 * ff] = (scaled * silu).astype(BF16)
        wt[rows_c, :] = (gate * hidden).astype(BF16)
        grads = gp[rows_c, :]
        theirs = wgu[pl.ds(pl.multiple_of(other * half, half), half), :]
        psend[...] = lax.dot_general(grads, theirs, NT, preferred_element_type=F32).astype(BF16)
        swap = remote(psend, precv.at[g], p_s, p_r.at[g], partner)
        swap.start()
        gps[...] = lax.dot_general(
            row_src, jnp.where(slot_mask, gate_part, 0.0), TN,
            preferred_element_type=F32, precision=HI,
        )
        swap_gate = remote(gps, gpr.at[g], pg_s, pg_r.at[g], partner)
        swap_gate.start()
        ours = wgu[pl.ds(pl.multiple_of(core * half, half), half), :]
        own[...] = lax.dot_general(grads, ours, NT, preferred_element_type=F32).astype(BF16)
        group_wait(g, d_copy(g, 0), False)
        group_wait(g, d_copy(g, 1), False)
        swap.wait()
        swap_gate.wait()

        def row_grad(k):
            cols = slice(k * CH, (k + 1) * CH)
            return (own[:, cols].astype(F32) + precv[g, :, cols].astype(F32)).astype(BF16)

        tail = row_grad(nk)
        for k in range(nk):
            part = mm(qm[0], row_grad(k)) + mm(qm[1 + k], tail)
            send[rows_w, k * CH : (k + 1) * CH] = part.astype(BF16)
        rgs[pl.ds(g * gs, gs)] = (gps[...] + gpr[g]).reshape(gs, 1, 128)

        @pl.when(g == 0)
        def _():
            back[0:16, :] = send[0:16, 0:fold]
            bg[0] = rgs[0]

        @pl.when(g == ng - 1)
        def _():
            send_back(g)

        return carry

    lax.fori_loop(0, ng, expert, 0)

    def grad_gu(i, carry):
        cols = pl.ds(pl.multiple_of(i * CH, CH), CH)
        g = lax.dot_general(xv[:, cols], gp[...], TN, preferred_element_type=F32).astype(BF16)
        wgu[cols, :] = g
        sq = g.astype(F32)
        sq = sq * sq
        ones = jnp.ones((8, ff), F32)
        sqs[0:8, cols] = lax.dot_general(ones, sq[:, :ff], NT, preferred_element_type=F32)
        sqs[8:16, cols] = lax.dot_general(ones, sq[:, ff:], NT, preferred_element_type=F32)
        return carry

    lax.fori_loop(0, width // CH, grad_gu, 0)
    sums = remote(sqs, sqr, sq_s, sq_r, partner)
    sums.start()
    sqa[...] = jnp.zeros_like(sqa)

    def grad_d(i, carry):
        cols = pl.ds(pl.multiple_of(i * CH, CH), CH)
        g = lax.dot_general(wt[...], yv[:, cols], TN, preferred_element_type=F32).astype(BF16)
        wd[:, cols] = g
        sq = g.astype(F32)
        sq = sq * sq
        acc = sq[:, 0:128]
        for k in range(1, CH // 128):
            acc += sq[:, k * 128 : (k + 1) * 128]
        sqa[...] += acc
        return carry

    lax.fori_loop(0, width // CH, grad_d, 0)
    sq_down = lax.dot_general(
        jnp.ones((8, 128), F32), sqa[...], NT, preferred_element_type=F32, precision=HI
    )
    sqd_o[...] = sq_down[0:1, :] * (1.0 / width)

    hot_c = [
        jnp.transpose(
            jnp.where(iota((n_pos, rows_tok), 0) == exp_r[j : j + 1, :], 1.0, 0.0)
        )
        for j in range(2)
    ]
    lower = hot(iota((rows_tok, rows_tok), 1) < iota((rows_tok, rows_tok), 0))
    prior_c = mm(lower, (hot_c[0] + hot_c[1]).astype(BF16))
    key_sub = [
        jnp.sum(
            hot_c[j] * (prior_c + 16.0 * iota((rows_tok, n_pos), 1).astype(F32)),
            axis=1, keepdims=True,
        ).astype(I32)
        for j in range(2)
    ]
    lane = iota((rows_tok, 16 * n_pos), 1)
    r = lane & 15
    base = expert_vec(lane >> 4) * 16
    direct = base + r
    folded = jnp.where(r >= CAP, base + r - CAP, -4096)
    homes = [(key_sub[0] == direct) | (key_sub[1] == direct)] + [
        (key_sub[0] == folded + 4 * k) | (key_sub[1] == folded + 4 * k) for k in range(nk)
    ]
    n_wire = 16 * n_pos
    for m in range(nk + 1):
        tokv[m // 2, :, (m % 2) * n_wire : (m % 2 + 1) * n_wire] = hot(homes[m])

    sums.wait()
    scale = 1.0 / (2 * ff)
    sqg_o[...] = (sqs[0:1, :] + sqr[0:1, :]) * scale
    squ_o[...] = (sqs[8:9, :] + sqr[8:9, :]) * scale

    def arrive(g, carry):
        group_wait(g, rg_copy(g), True)
        group_wait(g, r_copy(g), True)
        return carry

    lax.fori_loop(0, ng, arrive, 0)
    def drain(g, carry):
        group_wait(g, dg_copy(g), False)
        group_wait(g, rg_copy(g), False)
        group_wait(g, r_copy(g), False)
        return carry

    lax.fori_loop(0, ng, drain, 0)


def flush(
    wgu, wd, sqg, squ, sqd, back, bg, homes, slot, place,
    gt_o, gg_o, ggw_o, guw_o, gdw_o, sqg_o, squ_o, sqd_o, gtv, sem,
):
    ff = wd.shape[0]
    rows_tok = gtv.shape[0]
    n_wire, fold = back.shape
    nk = fold // CH
    part = wgu.shape[0] // 4
    pairs = [
        (wgu.at[i * part : (i + 1) * part, j * ff : (j + 1) * ff],
         (ggw_o, guw_o)[j].at[i * part : (i + 1) * part, :])
        for i in range(4) for j in range(2)
    ] + [
        (wd.at[i * (ff // 4) : (i + 1) * (ff // 4), :],
         gdw_o.at[i * (ff // 4) : (i + 1) * (ff // 4), :])
        for i in range(4)
    ] + [(sqg, sqg_o), (squ, squ_o), (sqd, sqd_o), (gtv, gt_o)]
    copies = [
        pltpu.make_async_copy(src, dst, sem.at[i]) for i, (src, dst) in enumerate(pairs)
    ]
    for copy in copies[:-1]:
        copy.start()

    def home(m):
        return homes[m // 2, :, (m % 2) * n_wire : (m % 2 + 1) * n_wire]

    tail = jnp.zeros((rows_tok, CH), F32)
    for k in range(nk):
        piece = back[:, k * CH : (k + 1) * CH]
        gtv[:, k * CH : (k + 1) * CH] = mm(home(0), piece).astype(BF16)
        tail += mm(home(1 + k), piece)
    gtv[:, fold : fold + CH] = tail.astype(BF16)
    copies[-1].start()
    back_gate = bg[...].reshape(bg.shape[0], 128)
    for j in range(2):
        rows = lax.dot_general(
            back_gate, place[j], TN, preferred_element_type=F32, precision=HI
        )
        gg_o[j : j + 1, :] = jnp.sum(
            jnp.where(iota((128, rows_tok), 0) == slot[j : j + 1, :], rows, 0.0),
            axis=0, keepdims=True,
        )
    for copy in copies:
        copy.wait()


GS = 16
RETURNS = ((3, (0, 1, 2)),)
VMEM_K1 = 48 * 2**20
VMEM_K2 = 6 * 2**20


def body(tokens, cotangent, gates, experts, gate_w, up_w, down_w):
    rows, width = tokens.shape
    half = width // 2
    ff = down_w.shape[1]
    n_pos = SIDE ** 3
    ng = n_pos // GS
    n_wire = 16 * n_pos
    n_rows = CAP * n_pos
    fold = half - CH
    wr, cr = 16 * GS, CAP * GS
    any_spec = pl.BlockSpec(memory_space=pl.ANY)
    vmem = pl.BlockSpec(memory_space=pltpu.VMEM)
    dma = pltpu.SemaphoreType.DMA
    outs = pl.pallas_call(
        functools.partial(kernel, GS),
        out_shape=(
            pltpu.VMEM((width, 2 * ff), BF16),
            pltpu.VMEM((ff, width), BF16),
            pltpu.VMEM((1, width), F32),
            pltpu.VMEM((1, width), F32),
            pltpu.VMEM((1, ff), F32),
            pltpu.VMEM((n_wire, fold), BF16),
            pltpu.VMEM((n_pos, 1, 128), F32),
            pltpu.VMEM((2, rows, half), BF16),
            pltpu.VMEM((2, rows), I32),
            pltpu.VMEM((2, n_pos, rows), F32),
        ),
        in_specs=[vmem, vmem] + [any_spec] * 5,
        out_specs=(vmem,) * 10,
        scratch_shapes=[
            pltpu.VMEM((n_wire, 2 * fold), BF16),
            pltpu.VMEM((2, n_wire, 2 * fold), BF16),
            pltpu.VMEM((n_rows, width), BF16),
            pltpu.VMEM((n_rows, width), BF16),
            pltpu.VMEM((n_rows, 2 * ff), BF16),
            pltpu.VMEM((n_rows, ff), BF16),
            pltpu.VMEM((cr, half), BF16),
            pltpu.VMEM((cr, half), BF16),
            pltpu.VMEM((ng, cr, half), BF16),
            pltpu.VMEM((4, cr, wr), BF16),
            pltpu.VMEM((4, wr, cr), BF16),
            pltpu.VMEM((n_pos, 1, 128), F32),
            pltpu.VMEM((n_pos, 1, 128), F32),
            pltpu.VMEM((GS, 128), F32),
            pltpu.VMEM((ng, GS, 128), F32),
            pltpu.VMEM((n_pos, 1, 128), F32),
            pltpu.VMEM((16, width), F32),
            pltpu.VMEM((16, width), F32),
            pltpu.VMEM((ff, 128), F32),
            dma((2 * ng,)), dma((2 * ng,)), dma((ng,)), dma((ng,)),
            dma((2,)), dma((2 * ng,)), dma, dma((ng,)), dma, dma((ng,)),
            dma((ng,)), dma((ng,)), dma((ng,)), dma((ng,)),
            dma, dma, dma((5,)),
        ],
        compiler_params=pltpu.CompilerParams(
            collective_id=0, has_side_effects=True, vmem_limit_bytes=VMEM_K1
        ),
    )(experts.T, gates.T, tokens, cotangent, gate_w[0], up_w[0], down_w[0])
    outs = pl.pallas_call(
        flush,
        out_shape=(
            jax.ShapeDtypeStruct((rows, half), BF16),
            jax.ShapeDtypeStruct((2, rows), F32),
            jax.ShapeDtypeStruct((width, ff), BF16),
            jax.ShapeDtypeStruct((width, ff), BF16),
            jax.ShapeDtypeStruct((ff, width), BF16),
            jax.ShapeDtypeStruct((1, width), F32),
            jax.ShapeDtypeStruct((1, width), F32),
            jax.ShapeDtypeStruct((1, ff), F32),
        ),
        in_specs=[vmem] * 10,
        out_specs=(any_spec, vmem) + (any_spec,) * 6,
        scratch_shapes=[pltpu.VMEM((rows, half), BF16), dma((16,))],
        compiler_params=pltpu.CompilerParams(vmem_limit_bytes=VMEM_K2),
    )(*outs)
    gt, gg, ggw, guw, gdw, sqg, squ, sqd = outs
    return gt, gg.T, ggw[None], guw[None], gdw[None], sqg, squ, sqd


def solution(mesh):
    placed = (
        P("ep", None),
        P("ep", None),
        P("ep", None),
        P("ep", None),
        P("ep", None, "tp"),
        P("ep", None, "tp"),
        P("ep", "tp", None),
    )
    return jax.shard_map(
        body,
        mesh=mesh,
        in_specs=placed,
        out_specs=(
            P("ep", "tp"),
            P("ep", None),
            P("ep", None, "tp"),
            P("ep", None, "tp"),
            P("ep", "tp", None),
            P("ep", None),
            P("ep", None),
            P("ep", "tp"),
        ),
        check_vma=False,
    )
```

time: 162 us -> 130 us (0.80)
  the two profiles are of different devices: /device:TPU:43 before, /device:TPU:88 now
where the time goes in v2:
time: 130 us
  Pallas kernels  129 us (99%)
    pallas_call x1, Pallas kernels, body(): pl.pallas_call(functools.partial(kernel, GS), out_shape=(pltpu.VMEM((widt...  124 us
    pallas_call x1, Pallas kernels, body(): pl.pallas_call(flush, out_shape=(jax.ShapeDtypeStruct((rows, half), BF16)...  5.3 us

profile of v2, /device:TPU:88, one launch (start us, length us, event | category | flops | bytes accessed | tf_op | source)
XLA Modules:
  0.0 129.9 jit_solution(16241283228394093393)
XLA Ops:
  0.6 123.9 %shard_map.134 = (bf16[4096,768]{1,0:T(8,128)(2,1)S(1)}, bf16[384,4096]{1,0:T(8,128)(2,1)S(1)}, f32[1,4096]{1,0:T(1,128)S(1)}, f32[1,4096]{1,0:T(1,128)S(1)}, f3...) custom-call(s32[2,256]{1,0:T(2,128)} %bitcast.12, ...), custom_call_target="tpu_custom_call" | custom-call | tf_op jit(solution)/shard_map/pallas_call | solution.py:542
  124.6 5.3 %shard_map.135 = (bf16[256,2048]{1,0:T(8,128)(2,1)}, f32[2,256]{1,0:T(2,128)}, bf16[4096,384]{1,0:T(8,128)(2,1)}, bf16[4096,384]{1,0:T(8,128)(2,1)}, bf16[384,40...) custom-call(bf16[4096,768]{1,0:T(8,128)(2,1)S(1)} %get-tuple-element.26.wgu, ...), custom_call_target="tpu_custom_call" | custom-call | tf_op jit(solution)/shard_map/pallas_call | solution.py:587

commit v3 on v2

--- a/solution.py
+++ b/solution.py
@@ -490,11 +490,14 @@
         (wd.at[i * (ff // 4) : (i + 1) * (ff // 4), :],
          gdw_o.at[i * (ff // 4) : (i + 1) * (ff // 4), :])
         for i in range(4)
-    ] + [(sqg, sqg_o), (squ, squ_o), (sqd, sqd_o), (gtv, gt_o)]
+    ] + [(sqg, sqg_o), (squ, squ_o), (sqd, sqd_o)] + [
+        (gtv.at[:, k * CH : (k + 1) * CH], gt_o.at[:, k * CH : (k + 1) * CH])
+        for k in range(nk + 1)
+    ]
     copies = [
         pltpu.make_async_copy(src, dst, sem.at[i]) for i, (src, dst) in enumerate(pairs)
     ]
-    for copy in copies[:-1]:
+    for copy in copies[: -nk - 1]:
         copy.start()
 
     def home(m):
@@ -505,6 +508,7 @@
         piece = back[:, k * CH : (k + 1) * CH]
         gtv[:, k * CH : (k + 1) * CH] = mm(home(0), piece).astype(BF16)
         tail += mm(home(1 + k), piece)
+        copies[k - nk - 1].start()
     gtv[:, fold : fold + CH] = tail.astype(BF16)
     copies[-1].start()
     back_gate = bg[...].reshape(bg.shape[0], 128)
@@ -598,7 +602,7 @@
         ),
         in_specs=[vmem] * 10,
         out_specs=(any_spec, vmem) + (any_spec,) * 6,
-        scratch_shapes=[pltpu.VMEM((rows, half), BF16), dma((16,))],
+        scratch_shapes=[pltpu.VMEM((rows, half), BF16), dma((19,))],
         compiler_params=pltpu.CompilerParams(vmem_limit_bytes=VMEM_K2),
     )(*outs)
     gt, gg, ggw, guw, gdw, sqg, squ, sqd = outs

time: 130 us -> 130 us (level)
  no operation moved by 1% of the time
where the time goes in v3:
time: 130 us; the launch traced here: 129 us
  Pallas kernels  129 us (99%)
    pallas_call x1, Pallas kernels, body(): pl.pallas_call(functools.partial(kernel, GS), out_shape=(pltpu.VMEM((widt...  124 us
    pallas_call x1, Pallas kernels, body(): pl.pallas_call(flush, out_shape=(jax.ShapeDtypeStruct((rows, half), BF16)...  4.85 us

profile of v3, /device:TPU:88, one launch (start us, length us, event | category | flops | bytes accessed | tf_op | source)
XLA Modules:
  0.0 129.4 jit_solution(3948772134396865233)
XLA Ops:
  0.6 123.9 %shard_map.134 = (bf16[4096,768]{1,0:T(8,128)(2,1)S(1)}, bf16[384,4096]{1,0:T(8,128)(2,1)S(1)}, f32[1,4096]{1,0:T(1,128)S(1)}, f32[1,4096]{1,0:T(1,128)S(1)}, f3...) custom-call(s32[2,256]{1,0:T(2,128)} %bitcast.12, ...), custom_call_target="tpu_custom_call" | custom-call | tf_op jit(solution)/shard_map/pallas_call | solution.py:546
  124.6 4.9 %shard_map.135 = (bf16[256,2048]{1,0:T(8,128)(2,1)}, f32[2,256]{1,0:T(2,128)}, bf16[4096,384]{1,0:T(8,128)(2,1)}, bf16[4096,384]{1,0:T(8,128)(2,1)}, bf16[384,40...) custom-call(bf16[4096,768]{1,0:T(8,128)(2,1)S(1)} %get-tuple-element.26.wgu, ...), custom_call_target="tpu_custom_call" | custom-call | tf_op jit(solution)/shard_map/pallas_call | solution.py:591
